TPU v7x, 32 devices: a whole 2x2x4 slice. The times are simulated.
32 devices in a mesh: sp: 16 (over z, y, x), tp: 2 (over core).
Axes of the slice: x: 2, y: 2, z: 4, core: 2. Of those that a mesh axis runs over, the one named last changes fastest.
Arguments:
- residual: bfloat16 [4096, 2048], P('sp'), may hold values from -6 to 6
- queries: bfloat16 [4096, 1024], P('sp', 'tp'), may hold values from -6 to 6
- forget_gate_logits: bfloat16 [4096, 1024], P('sp', 'tp'), may hold values from -5 to 5
- projected_values: bfloat16 [4096, 1024], P('sp', 'tp'), may hold values from -6 to 6
- output_gate_logits: bfloat16 [4096, 1024], P('sp', 'tp'), may hold values from -6 to 6
- lower_bound_margin: float32 [1024], P('tp'), may hold values from 0.00024414062 to 0.08
- extra_forget_logs: float32 [4096, 1024], P('sp', 'tp'), may hold values from -0.7 to 0
- per_head_norm_gain: float32 [128], replicated, may hold values from 0.1 to 1.9
- output_weight: bfloat16 [1024, 2048], P('tp'), may hold values from -0.1875 to 0.1875
- feedforward_norm_gain: float32 [2048], replicated, may hold values from 0.1 to 1.9
- gate_weight: bfloat16 [2048, 5632], P('sp', 'tp'), may hold values from -0.125 to 0.125
- up_weight: bfloat16 [2048, 5632], P('sp', 'tp'), may hold values from -0.125 to 0.125
- down_weight: bfloat16 [5632, 2048], P('tp', 'sp'), may hold values from -0.078125 to 0.078125
Outputs:
- layer_out: bfloat16 [4096, 2048], P('sp')
All inputs are finite; a program needn't handle non-finite values.
Results may differ from a plain program's by a relative error of at most 0.015.
Values may be sent and summed in bfloat16 or wider, within the bound.
A program may use at most 128 MiB of HBM per device.

v0:
```python
import jax
import jax.numpy as jnp
from jax import lax
from jax.sharding import PartitionSpec as P

HD = 128
BLOCK = 64


eps = 1e-06
top_precision = lax.Precision.HIGHEST


def carried_in_2(value, axis, join, neutral):
    place = lax.axis_index(axis)
    gathered = jax.tree.map(
        lambda a, kind: lax.all_gather(a.astype(kind), axis), value, (jnp.bfloat16, jnp.bfloat16)
    )
    state = jax.tree.map(lambda a, e: jnp.zeros_like(a) + jnp.asarray(e, a.dtype), value, neutral)

    def one(turn, state):
        return join(
            state,
            jax.tree.map(
                lambda a, own: lax.dynamic_index_in_dim(a, turn, 0, False).astype(own.dtype),
                gathered,
                value,
            ),
        )

    return lax.fori_loop(0, place, one, state)


def block_update(carried_in, inputs):
    recurrent_state, offset = carried_in
    queries, state_increment, value_rows, retain_log_factor = inputs
    running_state = jnp.cumsum(retain_log_factor, axis=1)
    causal = jnp.tril(
        jnp.ones((retain_log_factor.shape[1], retain_log_factor.shape[1]), dtype=bool)
    )
    carried_over_state = jnp.einsum(
        "uqw,uwa->uqa", queries * jnp.exp(running_state), recurrent_state, precision=top_precision
    )
    spread = running_state[:, :, None, :] - running_state[:, None, :, :]
    weights = jnp.exp(jnp.where(causal[None, :, :, None], spread, -jnp.inf))
    scores = jnp.einsum(
        "htk,htsk,hsk->hts", queries, weights, state_increment, precision=top_precision
    )
    output_rows = carried_over_state + jnp.einsum(
        "hts,hsv->htv", scores, value_rows, precision=top_precision
    )
    final_state = running_state[:, -1:, :]
    updated_state = jnp.exp(final_state[:, 0, :])[:, :, None] * recurrent_state + jnp.einsum(
        "erb,erc->ebc",
        state_increment * jnp.exp(final_state - running_state),
        value_rows,
        precision=top_precision,
    )
    rescaled_state = queries * jnp.exp(running_state + offset[:, None, :])
    return ((updated_state, offset + final_state[:, 0, :]), (output_rows, rescaled_state))


def join_states(earlier, later):
    earlier_sum, earlier_memory = earlier
    later_sum, later_memory = later
    return (earlier_sum + later_sum, jnp.exp(later_sum)[:, :, None] * earlier_memory + later_memory)


def local(
    residual,
    queries,
    forget_gate_logits,
    projected_values,
    output_gate_logits,
    lower_bound_margin,
    extra_forget_logs,
    per_head_norm_gain,
    output_weight,
    feedforward_norm_gain,
    gate_weight,
    up_weight,
    down_weight,
):
    length = queries.shape[0]
    head_count = queries.shape[1] // HD
    state_increment = lower_bound_margin * jax.nn.sigmoid(-forget_gate_logits.astype(jnp.float32))
    retain_log_factor = jnp.log1p(-state_increment) + extra_forget_logs

    def to_blocks(source):
        return source.reshape(length // BLOCK, BLOCK, head_count, HD).transpose(0, 2, 1, 3)

    initial = (
        jnp.zeros((head_count, HD, HD), jnp.float32),
        jnp.zeros((head_count, HD), jnp.float32),
    )
    block_inputs = (
        to_blocks(queries.astype(jnp.float32)),
        to_blocks(state_increment),
        to_blocks(projected_values.astype(jnp.float32)),
        to_blocks(retain_log_factor),
    )
    (recurrent_state, decay_sum), (output_rows, rescaled_state) = lax.scan(
        block_update, initial, block_inputs
    )
    identity = (jnp.zeros_like(decay_sum), jnp.zeros_like(recurrent_state))
    incoming_state = carried_in_2((decay_sum, recurrent_state), "sp", join_states, identity)[1]
    output_rows = output_rows + jnp.einsum(
        "sjey,jyx->sjex", rescaled_state, incoming_state, precision=top_precision
    )
    mixed = output_rows.transpose(0, 2, 1, 3).reshape(length, head_count, HD)
    normed_heads = (
        mixed
        * lax.rsqrt(jnp.mean(mixed * mixed, axis=-1, keepdims=True) + eps)
        * per_head_norm_gain
    )
    gating = jax.nn.silu(output_gate_logits.astype(jnp.float32)).reshape(length, head_count, HD)
    gated = (normed_heads * gating).reshape(length, head_count * HD).astype(jnp.bfloat16)
    row_count = residual.shape[0] // lax.axis_size("tp")
    own_rows = lax.dynamic_slice_in_dim(residual, lax.axis_index("tp") * row_count, row_count, 0)
    rows_here = gated
    projected = lax.psum_scatter(
        jnp.dot(rows_here, output_weight, preferred_element_type=jnp.float32).astype(jnp.bfloat16),
        "tp",
        scatter_dimension=0,
        tiled=True,
    ).astype(jnp.float32)
    after_mixer = (own_rows.astype(jnp.float32) + projected).astype(jnp.bfloat16)
    widened = after_mixer.astype(jnp.float32)
    normed = (
        widened
        * lax.rsqrt(jnp.mean(widened * widened, axis=-1, keepdims=True) + eps)
        * feedforward_norm_gain
    ).astype(jnp.bfloat16)
    gate_full, up_full = (
        lax.all_gather(gate_weight, "sp", axis=0, tiled=True),
        lax.all_gather(up_weight, "sp", axis=0, tiled=True),
    )
    down_full = lax.all_gather(down_weight, "sp", axis=1, tiled=True)
    row_piece = lax.all_gather(normed, "tp", axis=0, tiled=True)
    gate_part = jnp.dot(row_piece, gate_full, preferred_element_type=jnp.float32)
    up_part = jnp.dot(row_piece, up_full, preferred_element_type=jnp.float32)
    hidden = (jax.nn.silu(gate_part) * up_part).astype(jnp.bfloat16)
    rows_here = hidden
    ffn_sum = lax.psum_scatter(
        jnp.dot(rows_here, down_full, preferred_element_type=jnp.float32).astype(jnp.bfloat16),
        "tp",
        scatter_dimension=0,
        tiled=True,
    ).astype(jnp.float32)
    finished = (after_mixer.astype(jnp.float32) + 0.5 * ffn_sum).astype(jnp.bfloat16)
    return lax.all_gather(finished, "tp", axis=0, tiled=True)


def solution(mesh):
    return jax.shard_map(
        local,
        mesh=mesh,
        in_specs=(
            P("sp", None),
            P("sp", "tp"),
            P("sp", "tp"),
            P("sp", "tp"),
            P("sp", "tp"),
            P("tp"),
            P("sp", "tp"),
            P(),
            P("tp", None),
            P(),
            P("sp", "tp"),
            P("sp", "tp"),
            P("tp", "sp"),
        ),
        out_specs=P("sp", None),
        check_vma=False,
    )
```

profile of v0, /device:TPU:0, one launch (start us, length us, event | category | flops | bytes accessed | tf_op | source)
XLA Modules:
  0.0 711.4 jit_solution(5645837955671285264)
XLA Ops:
  6.5 2.4 divide_multiply_fusion
  11.1 1.9 reshape.91
  13.0 1.9 reshape.92
  15.0 75.4 %while.30 = (s32[]{:T(128)}, f32[4,128,128]{2,1,0:T(8,128)S(1)}, f32[4,128]{1,0:T(4,128)S(1)}, f32[4,4,64,128]{3,2,0,1:T(8,128)}, f32[4,4,64,128]{3,2,0,1:T(8,12...) while((s32[]{:T(128)}, f32[4,128,128]{2,1,0:T(8,128)S(1)}, ...), condition=%wide.region_2.3_spmd.clone, body=%wide.region_0.2_spmd.clone.sunk | while | flops 159814656 | bytes 5010573 | solution.py:102
  17.1 14.1 %fusion.72 = f32[4,64,1,64]{3,2,1,0:T(1,128)S(1)} fusion(f32[4,64,128,1]{2,3,1,0:T(1,128)S(1)} %bitcast.133, f32[4,64,128]{2,1,0:T(8,128)S(1)} %bitcast.134, f32[4,64,128]{2,1,0:T(8,128)S(1)} %reduce_window_sum.16, pred[64,64]{1,0:T(8,128)(4,1)S(1)} %iota_compare_fusion.2), kind=kOutput, calls=%fused_computation.2.clone.1 | convolution fusion | flops 31457280 | bytes 462848 | tf_op jit(solution)/shard_map/while/body/eval_jaxpr/htk,htsk,hsk->hts/dot_general | solution.py:46
  35.9 14.1 %fusion.72 = f32[4,64,1,64]{3,2,1,0:T(1,128)S(1)} fusion(f32[4,64,128,1]{2,3,1,0:T(1,128)S(1)} %bitcast.133, f32[4,64,128]{2,1,0:T(8,128)S(1)} %bitcast.134, f32[4,64,128]{2,1,0:T(8,128)S(1)} %reduce_window_sum.16, pred[64,64]{1,0:T(8,128)(4,1)S(1)} %iota_compare_fusion.2), kind=kOutput, calls=%fused_computation.2.clone.1 | convolution fusion | flops 31457280 | bytes 462848 | tf_op jit(solution)/shard_map/while/body/eval_jaxpr/htk,htsk,hsk->hts/dot_general | solution.py:46
  54.8 14.1 %fusion.72 = f32[4,64,1,64]{3,2,1,0:T(1,128)S(1)} fusion(f32[4,64,128,1]{2,3,1,0:T(1,128)S(1)} %bitcast.133, f32[4,64,128]{2,1,0:T(8,128)S(1)} %bitcast.134, f32[4,64,128]{2,1,0:T(8,128)S(1)} %reduce_window_sum.16, pred[64,64]{1,0:T(8,128)(4,1)S(1)} %iota_compare_fusion.2), kind=kOutput, calls=%fused_computation.2.clone.1 | convolution fusion | flops 31457280 | bytes 462848 | tf_op jit(solution)/shard_map/while/body/eval_jaxpr/htk,htsk,hsk->hts/dot_general | solution.py:46
  73.6 14.1 %fusion.72 = f32[4,64,1,64]{3,2,1,0:T(1,128)S(1)} fusion(f32[4,64,128,1]{2,3,1,0:T(1,128)S(1)} %bitcast.133, f32[4,64,128]{2,1,0:T(8,128)S(1)} %bitcast.134, f32[4,64,128]{2,1,0:T(8,128)S(1)} %reduce_window_sum.16, pred[64,64]{1,0:T(8,128)(4,1)S(1)} %iota_compare_fusion.2), kind=kOutput, calls=%fused_computation.2.clone.1 | convolution fusion | flops 31457280 | bytes 462848 | tf_op jit(solution)/shard_map/while/body/eval_jaxpr/htk,htsk,hsk->hts/dot_general | solution.py:46
  91.1 42.6 %all-gather.2 = bf16[16,4,128]{2,1,0:T(4,128)(2,1)S(1)} all-gather(bf16[1,4,128]{2,1,0:T(4,128)(2,1)S(1)} %convert_bitcast_fusion), channel_id=2, replica_groups=mesh['sp'=16,'tp'=2] {'sp'}, dimensions={0}, use_global_device_ids=true | all-gather | bytes 17408 | tf_op jit(solution)/shard_map/all_gather | solution.py:17
  133.7 20.7 %all-gather.20.cloned.1.call-done = bf16[64,128,128]{2,1,0:T(8,128)(2,1)} async-done(((bf16[4,128,128]{2,1,0:T(8,128)(2,1)}), bf16[64,128,128]{2,1,0:T(8,128)(2,1)}) %all-gather.20.cloned.1.call-update) | async-done | bytes 2097168 | tf_op jit(solution)/shard_map/all_gather | solution.py:17
  154.4 1.8 multiply_reduce_fusion
  157.0 2.7 convolution_convert_fusion.1
  159.8 24.2 %reduce-scatter.3.cloned.1.call-done = bf16[128,2048]{1,0:T(8,128)(2,1)} async-done(((bf16[256,2048]{1,0:T(8,128)(2,1)}), bf16[128,2048]{1,0:T(8,128)(2,1)}) %reduce-scatter.3.cloned.1.call-update) | async-done | bytes 524304 | tf_op jit(solution)/shard_map/reduce_scatter | solution.py:121
  184.0 1.5 fusion.30
  188.3 8.6 %all-gather.10.cloned.1.call-done = bf16[256,2048]{1,0:T(8,128)(2,1)} async-done(((bf16[128,2048]{1,0:T(8,128)(2,1)}), bf16[256,2048]{1,0:T(8,128)(2,1)}) %all-gather.10.cloned.1.call-update) | async-done | bytes 1048592 | tf_op jit(solution)/shard_map/all_gather | solution.py:139
  196.9 145.2 %all-gather.12.cloned.1.call-done = bf16[2048,2816]{1,0:T(8,128)(2,1)} async-done(((bf16[128,2816]{1,0:T(8,128)(2,1)}), bf16[2048,2816]{1,0:T(8,128)(2,1)}) %all-gather.12.cloned.1.call-update) | async-done | bytes 11534352 | tf_op jit(solution)/shard_map/all_gather | solution.py:135
  342.2 9.4 %fusion.47 = f32[256,2816]{1,0:T(8,128)} fusion(bf16[256,2048]{1,0:T(8,128)(2,1)} %all-gather.10.cloned.1.call-done, bf16[2048,2816]{1,0:T(8,128)(2,1)} %all-gather.12.cloned.1.call-done), kind=kOutput, calls=%fused_computation.80 | convolution fusion | flops 2952790016 | bytes 15466496 | tf_op jit(solution)/shard_map/dot_general | solution.py:140
  351.6 132.9 %all-gather.14.cloned.1.call-done = bf16[2048,2816]{1,0:T(8,128)(2,1)} async-done(((bf16[128,2816]{1,0:T(8,128)(2,1)}), bf16[2048,2816]{1,0:T(8,128)(2,1)}) %all-gather.14.cloned.1.call-update) | async-done | bytes 11534352 | tf_op jit(solution)/shard_map/all_gather | solution.py:136
  484.4 182.8 %all-gather.16.cloned.1.call-done = bf16[2816,2048]{1,0:T(8,128)(2,1)} async-done(((bf16[2816,128]{1,0:T(8,128)(2,1)}), bf16[2816,2048]{1,0:T(8,128)(2,1)}) %all-gather.16.cloned.1.call-update) | async-done | bytes 11534352 | tf_op jit(solution)/shard_map/all_gather | solution.py:138
  667.2 15.8 %convolution_convert_fusion = bf16[256,2048]{1,0:T(8,128)(2,1)} fusion(bf16[2816,2048]{1,0:T(8,128)(2,1)} %all-gather.16.cloned.1.call-done, bf16[256,2048]{1,0:T(8,128)(2,1)} %all-gather.10.cloned.1.call-done, bf16[2048,2816]{1,0:T(8,128)(2,1)} %all-gather.14.cloned.1.call-done, f32[256,2816]{1,0:T(8,128)} %fusion.47), kind=kOutput, calls=%fused_computation.45 | convolution fusion | flops 5910429696 | bytes 28049408 | tf_op jit(solution)/shard_map/dot_general | solution.py:145
  683.1 6.7 reduce-scatter.5.cloned.1.call-done
  689.8 2.0 fusion.33
  691.8 10.4 %all-gather.18.cloned.1.call-done = bf16[256,2048]{1,0:T(8,128)(2,1)} async-done(((bf16[128,2048]{1,0:T(8,128)(2,1)}), bf16[256,2048]{1,0:T(8,128)(2,1)}) %all-gather.18.cloned.1.call-update) | async-done | bytes 1048592 | tf_op jit(solution)/shard_map/all_gather | solution.py:151
  702.2 2.3 copy.110
  (93 shorter events, 25.6 us)
Async XLA Ops:
  6.5 150.5 %copy-start = (bf16[512,2048]{1,0:T(8,128)(2,1)S(1)}, bf16[512,2048]{1,0:T(8,128)(2,1)}, u32[]{:S(2)}) copy-start(bf16[512,2048]{1,0:T(8,128)(2,1)} %param.25) | copy-start | bytes 6291460
  6.5 147.8 %all-gather.20.cloned.1.call-start = ((), (), s32[]{:S(2)}) async-start(), calls=%async_computation.9 | async-start | bytes 2228224 | tf_op jit(solution)/shard_map/all_gather | solution.py:17
  15.0 118.7 %copy-start.3 = (f32[128]{0:T(128)S(1)}, f32[128]{0:T(128)}, u32[]{:S(2)}) copy-start(f32[128]{0:T(128)} %param.24) | copy-start | bytes 1540
  90.4 64.0 %copy-start.1 = (f32[4,4,64,128]{3,2,0,1:T(8,128)S(1)}, f32[4,4,64,128]{3,2,0,1:T(8,128)}, u32[]{:S(2)}) copy-start(f32[4,4,64,128]{3,2,0,1:T(8,128)} %get-tuple-element.99) | copy-start | bytes 1572868
  91.1 93.0 %reduce-scatter.3.cloned.1.call-start = ((), (), s32[]{:S(2)}) async-start(), calls=%async_computation.2 | async-start | bytes 1572864 | tf_op jit(solution)/shard_map/reduce_scatter | solution.py:121
  157.0 28.5 %copy-start.2 = (f32[2048]{0:T(1024)S(1)}, f32[2048]{0:T(1024)}, u32[]{:S(2)}) copy-start(f32[2048]{0:T(1024)} %param.26) | copy-start | bytes 24580
  159.8 37.2 %all-gather.10.cloned.1.call-start = ((), (), s32[]{:S(2)}) async-start(), calls=%async_computation.3 | async-start | bytes 1572864 | tf_op jit(solution)/shard_map/all_gather | solution.py:139
  186.5 155.6 %all-gather.12.cloned.1.call-start = ((), (), s32[]{:S(2)}) async-start(), calls=%async_computation.4 | async-start | bytes 12255232 | tf_op jit(solution)/shard_map/all_gather | solution.py:135
  187.1 297.3 %all-gather.14.cloned.1.call-start = ((), (), s32[]{:S(2)}) async-start(), calls=%async_computation.5 | async-start | bytes 12255232 | tf_op jit(solution)/shard_map/all_gather | solution.py:136
  187.7 479.5 %all-gather.16.cloned.1.call-start = ((), (), s32[]{:S(2)}) async-start(), calls=%async_computation.6 | async-start | bytes 12255232 | tf_op jit(solution)/shard_map/all_gather | solution.py:138
  188.3 501.5 %reduce-scatter.5.cloned.1.call-start = ((), (), s32[]{:S(2)}) async-start(), calls=%async_computation.7 | async-start | bytes 1572864 | tf_op jit(solution)/shard_map/reduce_scatter | solution.py:144
  683.1 19.1 %all-gather.18.cloned.1.call-start = ((), (), s32[]{:S(2)}) async-start(), calls=%async_computation.8 | async-start | bytes 1572864 | tf_op jit(solution)/shard_map/all_gather | solution.py:151
Sparse Core Ops, SparseCore 0:
  91.2 63.1 all-gather.19
  159.9 24.0 reduce-scatter.2
  186.7 10.2 all-gather.9
  199.6 142.5 all-gather.11
  344.8 139.5 all-gather.13
  487.0 180.2 all-gather.15
  683.2 6.5 reduce-scatter.4
  691.9 10.2 all-gather.17
where the time goes:
time: 712 us; the launch traced here: 711 us
  waiting for transfers between devices  533 us (75%)
  matrix products  93.7 us (13%)
  blocking collectives  42.6 us (6%)
  local copies, waits for them, and re-layouts  16.9 us (2%)
  between operations  13.6 us (2%)
  other arithmetic  10.9 us (2%)
    all_gather x1, waiting for transfers between devices, local(): down_full = lax.all_gather(down_weight, 'sp', axis=1, tiled=True)  183 us
    all_gather x1, waiting for transfers between devices, local(): lax.all_gather(gate_weight, 'sp', axis=0, tiled=True)  145 us
    all_gather x1, waiting for transfers between devices, local(): lax.all_gather(up_weight, 'sp', axis=0, tiled=True)  133 us
    dot_general x4, matrix products, block_update(): jnp.einsum('htk,htsk,hsk->hts', queries, weights, state_increment, precis...  56.2 us
    all_gather x1, blocking collectives, carried_in_2(): lax.all_gather(a.astype(kind), axis)  42.6 us
    reduce_scatter x1, waiting for transfers between devices, local(): lax.psum_scatter(jnp.dot(rows_here, output_weight, preferred_element_type...  24.2 us
    all_gather x1, waiting for transfers between devices, carried_in_2(): lax.all_gather(a.astype(kind), axis)  20.7 us
    dot_general x1, matrix products, local(): jnp.dot(rows_here, down_full, preferred_element_type=jnp.float32)  15.8 us
  transfers between devices with their start and end apart: 8, of which 8 were waited for; matrix products, arithmetic and copies ran while one was open for 1% of the time, Pallas kernels for 0%

commit v1 on v0

--- a/solution.py
+++ b/solution.py
@@ -1,6 +1,8 @@
 import jax
 import jax.numpy as jnp
 from jax import lax
+from jax.experimental import pallas as pl
+from jax.experimental.pallas import tpu as pltpu
 from jax.sharding import PartitionSpec as P
 
 HD = 128
@@ -64,6 +66,196 @@
     earlier_sum, earlier_memory = earlier
     later_sum, later_memory = later
     return (earlier_sum + later_sum, jnp.exp(later_sum)[:, :, None] * earlier_memory + later_memory)
+
+
+MESH = pl.DeviceIdType.MESH
+GROUPS = 4
+
+
+def up_to(value, step):
+    return -(-value // step) * step
+
+
+def feed_forward_kernel(
+    dims, gu_ref, dn_ref, x_ref, nrm_ref, out_ref,
+    gu, dn, rows_in, hid, part, peer_part, summed, got,
+    s_a, r_a, s_b, r_b, s_x, r_x, s_p, r_p, s_d, r_d, s_r, r_r, s_o, r_o, s_l,
+):
+    n_r, share, own, width, padded = dims
+    me = lax.axis_index("sp")
+    c = lax.axis_index("tp")
+    h, r = me // n_r, me % n_r
+    model = gu.shape[0]
+
+    def away(d):
+        return (h + d) % GROUPS
+
+    def back(d):
+        return (h + GROUPS - d) % GROUPS
+
+    def beside(e):
+        return ((r // 2 + e // 2) % 2) * 2 + (r % 2 + e % 2) % 2
+
+    def remote(src, dst, send, recv, hh, rr, cc):
+        return pltpu.make_async_remote_copy(
+            src_ref=src, dst_ref=dst, send_sem=send, recv_sem=recv,
+            device_id=(hh * n_r + rr, cc), device_id_type=MESH,
+        )
+
+    def gu_rows(owner):
+        return gu.at[pl.ds(pl.multiple_of(owner * share, share), share)]
+
+    def dn_cols(owner):
+        return dn.at[pl.ds(0, width), pl.ds(pl.multiple_of(owner * share, share), share)]
+
+    def token_rows(hh, cc):
+        return pl.ds(pl.multiple_of((hh * 2 + cc) * own, own), own)
+
+    started = []
+
+    def go(copy):
+        copy.start()
+        started.append(copy)
+        return copy
+
+    weights_a = {}
+    weights_b = {}
+    for d in (1, 3, 2):
+        weights_a[d, 0] = go(remote(gu_ref.at[away(d)], gu_rows(me), s_a.at[d - 1, 0], r_a.at[d - 1, 0], away(d), r, c))
+    acts = {}
+    for d in (1, 3, 2):
+        acts[d] = go(remote(nrm_ref, rows_in.at[token_rows(h, c)], s_x.at[d - 1], r_x.at[d - 1], away(d), r, c))
+    peers = {0: go(remote(nrm_ref, rows_in.at[token_rows(h, c)], s_p.at[0], r_p.at[0], h, r, 1 - c))}
+    for d in (1, 3, 2):
+        weights_a[d, 1] = go(remote(dn_ref.at[away(d)], dn_cols(me), s_a.at[d - 1, 1], r_a.at[d - 1, 1], away(d), r, c))
+    own_gu = pltpu.make_async_copy(gu_ref.at[h], gu_rows(me), s_l.at[0])
+    own_dn = pltpu.make_async_copy(dn_ref.at[h], dn_cols(me), s_l.at[1])
+    own_gu.start()
+    own_dn.start()
+    for e in (1, 2, 3):
+        weights_b[0, e, 0] = go(remote(gu_ref.at[h], gu_rows(me), s_b.at[0, e - 1, 0], r_b.at[0, e - 1, 0], h, beside(e), c))
+    rows_in[token_rows(h, c), :] = nrm_ref[...]
+    dn[pl.ds(width, padded - width), :] = jnp.zeros((padded - width, model), dn.dtype)
+    for k in range(2):
+        if k == 1:
+            for e in (1, 2, 3):
+                weights_b[0, e, 1] = go(remote(dn_ref.at[h], dn_cols(me), s_b.at[0, e - 1, 1], r_b.at[0, e - 1, 1], h, beside(e), c))
+        for d in (1, 3, 2):
+            weights_a[d, k].wait_recv()
+            block = (gu_rows if k == 0 else dn_cols)(back(d) * n_r + r)
+            for e in (1, 2, 3):
+                weights_b[d, e, k] = go(remote(block, block, s_b.at[d, e - 1, k], r_b.at[d, e - 1, k], h, beside(e), c))
+        if k == 0:
+            for d in (1, 3, 2):
+                acts[d].wait_recv()
+                block = rows_in.at[token_rows(back(d), c)]
+                peers[d] = go(remote(block, block, s_p.at[d], r_p.at[d], h, r, 1 - c))
+    own_gu.wait()
+    own_dn.wait()
+    for d in range(4):
+        for e in (1, 2, 3):
+            weights_b[d, e, 0].wait_recv()
+
+    def reduce_block(d, exchange):
+        exchange.wait_recv()
+        here = part[d, pl.ds(pl.multiple_of(c * own, own), own), :]
+        total = here.astype(jnp.float32) + peer_part[d].astype(jnp.float32)
+        summed[d] = total.astype(jnp.bfloat16)
+        if d == 0:
+            return None
+        return go(remote(summed.at[d], got.at[d - 1], s_r.at[d - 1], r_r.at[d - 1], back(d), r, c))
+
+    tile = 256
+    order = (1, 3, 2, 0)
+    exchanges = {}
+    reduced = {}
+    for place, d in enumerate(order):
+        peers[d].wait_recv()
+        first = pl.multiple_of(back(d) * 2 * own, 2 * own)
+
+        def gate_up(j, carry):
+            at = pl.multiple_of(j * tile, tile)
+            rows = rows_in[pl.ds(first, 2 * own), :]
+            gate = jnp.dot(rows, gu[:, pl.ds(at, tile)], preferred_element_type=jnp.float32)
+            up = jnp.dot(rows, gu[:, pl.ds(padded + at, tile)], preferred_element_type=jnp.float32)
+            hid[:, pl.ds(at, tile)] = (gate * jax.nn.sigmoid(gate) * up).astype(jnp.bfloat16)
+            return carry
+
+        lax.fori_loop(0, padded // tile, gate_up, 0)
+        if place == 0:
+            for dd in range(4):
+                for e in (1, 2, 3):
+                    weights_b[dd, e, 1].wait_recv()
+
+        def down(j, carry):
+            at = pl.multiple_of(j * tile, tile)
+            part[d, :, pl.ds(at, tile)] = jnp.dot(
+                hid[...], dn[:, pl.ds(at, tile)], preferred_element_type=jnp.float32
+            ).astype(jnp.bfloat16)
+            return carry
+
+        lax.fori_loop(0, model // tile, down, 0)
+        exchanges[d] = go(remote(
+            part.at[d, pl.ds(pl.multiple_of((1 - c) * own, own), own)], peer_part.at[d],
+            s_d.at[d], r_d.at[d], h, r, 1 - c,
+        ))
+        if place:
+            reduced[order[place - 1]] = reduce_block(order[place - 1], exchanges[order[place - 1]])
+    reduce_block(0, exchanges[0])
+    total = summed[0].astype(jnp.float32)
+    for d in (1, 3, 2):
+        reduced[d].wait_recv()
+        total = total + got[d - 1].astype(jnp.float32)
+    mine = pl.ds(pl.multiple_of(c * own, own), own)
+    out_ref[mine, :] = (x_ref[...].astype(jnp.float32) + 0.5 * total).astype(jnp.bfloat16)
+    finish = go(remote(out_ref.at[mine], out_ref.at[mine], s_o.at[0], r_o.at[0], h, r, 1 - c))
+    finish.wait_recv()
+    for copy in started:
+        copy.wait_send()
+
+
+def feed_forward(gate_weight, up_weight, down_weight, after_mixer, normed):
+    n_sp = lax.axis_size("sp")
+    share, half = gate_weight.shape
+    width = half // GROUPS
+    padded = up_to(width, 256)
+    own, model = normed.shape
+    pad = ((0, 0), (0, 0), (0, padded - width))
+    split = lambda w: jnp.pad(w.reshape(share, GROUPS, width), pad)
+    gu = jnp.concatenate([split(gate_weight), split(up_weight)], axis=2).transpose(1, 0, 2)
+    dn = down_weight.reshape(GROUPS, width, share)
+    bf = jnp.bfloat16
+    dma = pltpu.SemaphoreType.DMA
+    dims = (n_sp // GROUPS, share, own, width, padded)
+    vm = pl.BlockSpec(memory_space=pltpu.VMEM)
+    hbm = pl.BlockSpec(memory_space=pl.ANY)
+    return pl.pallas_call(
+        lambda *refs: feed_forward_kernel(dims, *refs),
+        out_shape=jax.ShapeDtypeStruct((2 * own, model), bf),
+        in_specs=[hbm, hbm, vm, vm],
+        out_specs=vm,
+        scratch_shapes=[
+            pltpu.VMEM((model, 2 * padded), bf),
+            pltpu.VMEM((padded, model), bf),
+            pltpu.VMEM((GROUPS * 2 * own, model), bf),
+            pltpu.VMEM((2 * own, padded), bf),
+            pltpu.VMEM((GROUPS, 2 * own, model), bf),
+            pltpu.VMEM((GROUPS, own, model), bf),
+            pltpu.VMEM((GROUPS, own, model), bf),
+            pltpu.VMEM((GROUPS - 1, own, model), bf),
+            dma((3, 2)), dma((3, 2)), dma((4, 3, 2)), dma((4, 3, 2)),
+            dma((3,)), dma((3,)), dma((4,)), dma((4,)), dma((4,)), dma((4,)),
+            dma((3,)), dma((3,)), dma((1,)), dma((1,)), dma((2,)),
+        ],
+        compiler_params=pltpu.CompilerParams(has_side_effects=True, vmem_limit_bytes=56 * 2**20),
+    )(gu, dn, after_mixer, normed)
+
+
+def fits(mesh, share, own, width):
+    return (
+        mesh["sp"] == 4 * GROUPS and mesh["tp"] == 2
+        and share % 128 == 0 and own % 16 == 0 and width % 16 == 0
+    )
 
 
 def local(
@@ -131,6 +323,9 @@
         * lax.rsqrt(jnp.mean(widened * widened, axis=-1, keepdims=True) + eps)
         * feedforward_norm_gain
     ).astype(jnp.bfloat16)
+    sizes = {"sp": lax.axis_size("sp"), "tp": lax.axis_size("tp")}
+    if fits(sizes, gate_weight.shape[0], row_count, gate_weight.shape[1] // GROUPS):
+        return feed_forward(gate_weight, up_weight, down_weight, after_mixer, normed)
     gate_full, up_full = (
         lax.all_gather(gate_weight, "sp", axis=0, tiled=True),
         lax.all_gather(up_weight, "sp", axis=0, tiled=True),

time: 712 us -> 379 us (0.53)
  waiting for transfers between devices: 533 us -> 35.5 us
  Pallas kernels: 0 us -> 182 us
  matrix products: 93.7 us -> 68.6 us
    all_gather x5 -> x0, waiting for transfers between devices: 480 us -> none  [the longest x1 183 us: local(): down_full = lax.all_gather(down_weight, 'sp', axis=1, tiled=True)]
    pallas_call x0 -> x1, Pallas kernels: none -> 182 us  [feed_forward(): pl.pallas_call(lambda *refs: feed_forward_kernel(dims, *refs), out_shape=...]
    dot_general x2 -> x0, matrix products: 25.2 us -> none  [the longest x1 15.8 us: local(): jnp.dot(rows_here, down_full, preferred_element_type=jnp.float32)]
    reduce_scatter x1, waiting for transfers between devices: 24.2 us -> 14.8 us  [local(): lax.psum_scatter(jnp.dot(rows_here, output_weight, preferred_element_type...]
  transfers between devices with their start and end apart: 8 -> 2, of which waited for: 8 -> 2; matrix products, arithmetic and copies ran while one was open for 1% -> 3% of each run, Pallas kernels for 0% -> 0%
where the time goes in v1:
time: 379 us; the launch traced here: 378 us
  Pallas kernels  182 us (48%)
  matrix products  68.6 us (18%)
  blocking collectives  42.6 us (11%)
  waiting for transfers between devices  35.5 us (9%)
  local copies, waits for them, and re-layouts  24 us (6%)
  between operations  13.5 us (4%)
  other arithmetic  11.4 us (3%)
    pallas_call x1, Pallas kernels, feed_forward(): pl.pallas_call(lambda *refs: feed_forward_kernel(dims, *refs), out_shape=...  182 us
    dot_general x4, matrix products, block_update(): jnp.einsum('htk,htsk,hsk->hts', queries, weights, state_increment, precis...  56.2 us
    all_gather x1, blocking collectives, carried_in_2(): lax.all_gather(a.astype(kind), axis)  42.6 us
    all_gather x1, waiting for transfers between devices, carried_in_2(): lax.all_gather(a.astype(kind), axis)  20.7 us
    reduce_scatter x1, waiting for transfers between devices, local(): lax.psum_scatter(jnp.dot(rows_here, output_weight, preferred_element_type...  14.8 us
    dynamic_slice x20, local copies, waits for them, and re-layouts, local(): lax.scan(block_update, initial, block_inputs)  7.77 us
  transfers between devices with their start and end apart: 2, of which 2 were waited for; matrix products, arithmetic and copies ran while one was open for 3% of the time, Pallas kernels for 0%

profile of v1, /device:TPU:0, one launch (start us, length us, event | category | flops | bytes accessed | tf_op | source)
XLA Modules:
  0.0 377.9 jit_solution(5443511051057269000)
XLA Ops:
  6.5 2.4 divide_multiply_fusion
  8.9 1.2 reshape.97
  11.1 1.9 reshape.103
  13.0 1.9 reshape.104
  15.0 75.5 %while.30 = (s32[]{:T(128)}, f32[4,128,128]{2,1,0:T(8,128)S(1)}, f32[4,128]{1,0:T(4,128)S(1)}, f32[4,4,64,128]{3,2,0,1:T(8,128)}, f32[4,4,64,128]{3,2,0,1:T(8,12...) while((s32[]{:T(128)}, f32[4,128,128]{2,1,0:T(8,128)S(1)}, ...), condition=%wide.region_2.3_spmd.clone, body=%wide.region_0.2_spmd.clone.sunk | while | flops 159814656 | bytes 5010573 | solution.py:294
  17.1 14.1 %fusion.67 = f32[4,64,1,64]{3,2,1,0:T(1,128)S(1)} fusion(f32[4,64,128,1]{2,3,1,0:T(1,128)S(1)} %bitcast.133, f32[4,64,128]{2,1,0:T(8,128)S(1)} %bitcast.134, f32[4,64,128]{2,1,0:T(8,128)S(1)} %reduce_window_sum.16, pred[64,64]{1,0:T(8,128)(4,1)S(1)} %iota_compare_fusion.4), kind=kOutput, calls=%fused_computation.2.clone.1 | convolution fusion | flops 31457280 | bytes 462848 | tf_op jit(solution)/shard_map/while/body/eval_jaxpr/htk,htsk,hsk->hts/dot_general | solution.py:48
  31.4 1.0 fusion.69
  36.0 14.1 %fusion.67 = f32[4,64,1,64]{3,2,1,0:T(1,128)S(1)} fusion(f32[4,64,128,1]{2,3,1,0:T(1,128)S(1)} %bitcast.133, f32[4,64,128]{2,1,0:T(8,128)S(1)} %bitcast.134, f32[4,64,128]{2,1,0:T(8,128)S(1)} %reduce_window_sum.16, pred[64,64]{1,0:T(8,128)(4,1)S(1)} %iota_compare_fusion.4), kind=kOutput, calls=%fused_computation.2.clone.1 | convolution fusion | flops 31457280 | bytes 462848 | tf_op jit(solution)/shard_map/while/body/eval_jaxpr/htk,htsk,hsk->hts/dot_general | solution.py:48
  50.3 1.0 fusion.69
  54.8 14.1 %fusion.67 = f32[4,64,1,64]{3,2,1,0:T(1,128)S(1)} fusion(f32[4,64,128,1]{2,3,1,0:T(1,128)S(1)} %bitcast.133, f32[4,64,128]{2,1,0:T(8,128)S(1)} %bitcast.134, f32[4,64,128]{2,1,0:T(8,128)S(1)} %reduce_window_sum.16, pred[64,64]{1,0:T(8,128)(4,1)S(1)} %iota_compare_fusion.4), kind=kOutput, calls=%fused_computation.2.clone.1 | convolution fusion | flops 31457280 | bytes 462848 | tf_op jit(solution)/shard_map/while/body/eval_jaxpr/htk,htsk,hsk->hts/dot_general | solution.py:48
  73.7 14.1 %fusion.67 = f32[4,64,1,64]{3,2,1,0:T(1,128)S(1)} fusion(f32[4,64,128,1]{2,3,1,0:T(1,128)S(1)} %bitcast.133, f32[4,64,128]{2,1,0:T(8,128)S(1)} %bitcast.134, f32[4,64,128]{2,1,0:T(8,128)S(1)} %reduce_window_sum.16, pred[64,64]{1,0:T(8,128)(4,1)S(1)} %iota_compare_fusion.4), kind=kOutput, calls=%fused_computation.2.clone.1 | convolution fusion | flops 31457280 | bytes 462848 | tf_op jit(solution)/shard_map/while/body/eval_jaxpr/htk,htsk,hsk->hts/dot_general | solution.py:48
  91.2 42.6 %all-gather.2 = bf16[16,4,128]{2,1,0:T(4,128)(2,1)S(1)} all-gather(bf16[1,4,128]{2,1,0:T(4,128)(2,1)S(1)} %convert_bitcast_fusion), channel_id=2, replica_groups=mesh['sp'=16,'tp'=2] {'sp'}, dimensions={0}, use_global_device_ids=true | all-gather | bytes 17408 | tf_op jit(solution)/shard_map/all_gather | solution.py:19
  133.8 20.7 %all-gather.5.cloned.1.call-done = bf16[64,128,128]{2,1,0:T(8,128)(2,1)} async-done(((bf16[4,128,128]{2,1,0:T(8,128)(2,1)}), bf16[64,128,128]{2,1,0:T(8,128)(2,1)}) %all-gather.5.cloned.1.call-update) | async-done | bytes 2097168 | tf_op jit(solution)/shard_map/all_gather | solution.py:19
  154.5 1.8 multiply_reduce_fusion
  157.1 2.8 convolution_convert_fusion
  159.9 1.1 copy.27
  161.1 1.4 copy.28
  162.4 2.2 copy.29
  164.7 2.3 copy.30
  167.0 2.4 fusion.30.refs_0_
  169.4 14.8 %reduce-scatter.2.cloned.1.call-done = bf16[128,2048]{1,0:T(8,128)(2,1)} async-done(((bf16[256,2048]{1,0:T(8,128)(2,1)}), bf16[128,2048]{1,0:T(8,128)(2,1)}) %reduce-scatter.2.cloned.1.call-update) | async-done | bytes 524304 | tf_op jit(solution)/shard_map/reduce_scatter | solution.py:313
  184.2 1.5 fusion.33
  186.7 182.1 %shard_map.127 = bf16[256,2048]{1,0:T(8,128)(2,1)} custom-call(bf16[4,128,1536]{2,1,0:T(8,128)(2,1)} %fusion.30.refs_0_, bf16[4,704,128]{2,1,0:T(8,128)(2,1)} %bitcast.140, bf16[128,2048]{1,0:T(8,128)(2,1)} %copy-done.1, bf16[128,2048]{1,0:T(8,128)(2,1)} %fusion.35.refs_3_), custom_call_target="tpu_custom_call" | custom-call | tf_op jit(solution)/shard_map/pallas_call | solution.py:232
  368.8 2.3 copy.118
  (82 shorter events, 20.5 us)
Async XLA Ops:
  6.5 150.5 %copy-start = (bf16[512,2048]{1,0:T(8,128)(2,1)S(1)}, bf16[512,2048]{1,0:T(8,128)(2,1)}, u32[]{:S(2)}) copy-start(bf16[512,2048]{1,0:T(8,128)(2,1)} %param.25) | copy-start | bytes 6291460
  6.5 147.9 %all-gather.5.cloned.1.call-start = ((), (), s32[]{:S(2)}) async-start(), calls=%async_computation.2 | async-start | bytes 2228224 | tf_op jit(solution)/shard_map/all_gather | solution.py:19
  15.0 118.8 %copy-start.5 = (f32[128]{0:T(128)S(1)}, f32[128]{0:T(128)}, u32[]{:S(2)}) copy-start(f32[128]{0:T(128)} %param.24) | copy-start | bytes 1540
  90.4 64.0 %copy-start.3 = (f32[4,4,64,128]{3,2,0,1:T(8,128)S(1)}, f32[4,4,64,128]{3,2,0,1:T(8,128)}, u32[]{:S(2)}) copy-start(f32[4,4,64,128]{3,2,0,1:T(8,128)} %get-tuple-element.99) | copy-start | bytes 1572868
  91.1 93.0 %reduce-scatter.2.cloned.1.call-start = ((), (), s32[]{:S(2)}) async-start(), calls=%async_computation.1 | async-start | bytes 1572864 | tf_op jit(solution)/shard_map/reduce_scatter | solution.py:313
  157.1 2.8 copy-start.2
  167.0 18.7 %copy-start.4 = (f32[2048]{0:T(1024)S(1)}, f32[2048]{0:T(1024)}, u32[]{:S(2)}) copy-start(f32[2048]{0:T(1024)} %param.26) | copy-start | bytes 24580
  185.6 1.0 copy-start.1
Sparse Core Ops, SparseCore 0:
  91.3 63.1 all-gather.4
  160.0 24.0 reduce-scatter.1

commit v2 on v1

--- a/solution.py
+++ b/solution.py
@@ -76,10 +76,12 @@
     return -(-value // step) * step
 
 
-def feed_forward_kernel(
-    dims, gu_ref, dn_ref, x_ref, nrm_ref, out_ref,
-    gu, dn, rows_in, hid, part, peer_part, summed, got,
+def layer_kernel(
+    dims, gu_ref, dn_ref, q_ref, f_ref, v_ref, og_ref, margin_ref, extra_ref, head_gain_ref, ow_ref,
+    residual_ref, ff_gain_ref, out_ref,
+    gu, dn, grown, q_grown, plane, columns, gated, proj, proj_got, x_own, rows_in, hid, part, peer_part, summed, got,
     s_a, r_a, s_b, r_b, s_x, r_x, s_p, r_p, s_d, r_d, s_r, r_r, s_o, r_o, s_l,
+    s_1, r_1, s_2, r_2, s_j, r_j,
 ):
     n_r, share, own, width, padded = dims
     me = lax.axis_index("sp")
@@ -120,36 +122,133 @@
 
     weights_a = {}
     weights_b = {}
-    for d in (1, 3, 2):
-        weights_a[d, 0] = go(remote(gu_ref.at[away(d)], gu_rows(me), s_a.at[d - 1, 0], r_a.at[d - 1, 0], away(d), r, c))
-    acts = {}
-    for d in (1, 3, 2):
-        acts[d] = go(remote(nrm_ref, rows_in.at[token_rows(h, c)], s_x.at[d - 1], r_x.at[d - 1], away(d), r, c))
-    peers = {0: go(remote(nrm_ref, rows_in.at[token_rows(h, c)], s_p.at[0], r_p.at[0], h, r, 1 - c))}
-    for d in (1, 3, 2):
-        weights_a[d, 1] = go(remote(dn_ref.at[away(d)], dn_cols(me), s_a.at[d - 1, 1], r_a.at[d - 1, 1], away(d), r, c))
+    mine = pl.ds(pl.multiple_of(c * own, own), own)
+    theirs = pl.ds(pl.multiple_of((1 - c) * own, own), own)
+
+    def share_out(k):
+        source = (gu_ref, dn_ref)[k]
+        place = (gu_rows, dn_cols)[k]
+        for d in (1, 3, 2):
+            weights_a[d, k] = go(remote(source.at[away(d)], place(me), s_a.at[d - 1, k], r_a.at[d - 1, k], away(d), r, c))
+        for e in (1, 2, 3):
+            weights_b[0, e, k] = go(remote(source.at[h], place(me), s_b.at[0, e - 1, k], r_b.at[0, e - 1, k], h, beside(e), c))
+
+    def hand_on(d, k):
+        weights_a[d, k].wait_recv()
+        block = (gu_rows, dn_cols)[k](back(d) * n_r + r)
+        for e in (1, 2, 3):
+            weights_b[d, e, k] = go(remote(block, block, s_b.at[d, e - 1, k], r_b.at[d, e - 1, k], h, beside(e), c))
+
+    share_out(0)
     own_gu = pltpu.make_async_copy(gu_ref.at[h], gu_rows(me), s_l.at[0])
     own_dn = pltpu.make_async_copy(dn_ref.at[h], dn_cols(me), s_l.at[1])
     own_gu.start()
     own_dn.start()
+    dn[pl.ds(width, padded - width), :] = jnp.zeros((padded - width, model), dn.dtype)
+
+    bf, f32 = jnp.bfloat16, jnp.float32
+    length, channels = q_ref.shape
+    heads = channels // HD
+    span = 128
+    ones = lambda n: lax.broadcasted_iota(jnp.int32, (n, n), 0) >= lax.broadcasted_iota(jnp.int32, (n, n), 1)
+    lower = ones(length).astype(f32)
+    causal = ones(span)
+    over = lambda x, y, i, j: lax.dot_general(x, y, (((i,), (j,)), ((), ())), preferred_element_type=f32)
+    for n in range(heads):
+        cols = slice(n * HD, (n + 1) * HD)
+        inflow = margin_ref[:, cols] * jax.nn.sigmoid(-f_ref[:, cols].astype(f32))
+        keep = jnp.log1p(-inflow) + extra_ref[:, cols]
+        total_log = lax.dot_general(lower, keep, (((1,), (0,)), ((), ())), precision=top_precision, preferred_element_type=f32)
+        q = q_ref[:, cols].astype(f32)
+        q_grown[:, cols] = (q * jnp.exp(total_log)).astype(bf)
+        state = None
+        for start in range(0, length, span):
+            rows = slice(start, start + span)
+            a, qb, ub, vb = total_log[rows], q[rows], inflow[rows], v_ref[rows, cols]
+            middle, end = a[span // 2 - 1:span // 2], a[span - 1:span]
+            scores = over((qb * jnp.exp(a - middle)).astype(bf), (ub * jnp.exp(middle - a)).astype(bf), 1, 1)
+            mixed = over(jnp.where(causal, scores, 0.0).astype(bf), vb, 1, 0)
+            added = over(vb, (ub * jnp.exp(end - a)).astype(bf), 0, 0)
+            if state is None:
+                state = added
+            else:
+                mixed = mixed + over((qb * jnp.exp(a - base)).astype(bf), state.astype(bf), 1, 1)
+                state = state * jnp.exp(end - base) + added
+            grown[rows, cols] = mixed
+            base = end
+        plane[r, n * HD:(n + 1) * HD, :] = state.astype(bf)
+        high = base.astype(bf)
+        plane[r, heads * HD + n:heads * HD + n + 1, :] = high
+        plane[r, heads * HD + 8 + n:heads * HD + 9 + n, :] = (base - high.astype(f32)).astype(bf)
+
+    across = {e: go(remote(plane.at[r], plane.at[r], s_1.at[e - 1], r_1.at[e - 1], h, beside(e), c)) for e in (1, 2, 3)}
+    hand_on(1, 0)
     for e in (1, 2, 3):
-        weights_b[0, e, 0] = go(remote(gu_ref.at[h], gu_rows(me), s_b.at[0, e - 1, 0], r_b.at[0, e - 1, 0], h, beside(e), c))
-    rows_in[token_rows(h, c), :] = nrm_ref[...]
-    dn[pl.ds(width, padded - width), :] = jnp.zeros((padded - width, model), dn.dtype)
-    for k in range(2):
-        if k == 1:
-            for e in (1, 2, 3):
-                weights_b[0, e, 1] = go(remote(dn_ref.at[h], dn_cols(me), s_b.at[0, e - 1, 1], r_b.at[0, e - 1, 1], h, beside(e), c))
-        for d in (1, 3, 2):
-            weights_a[d, k].wait_recv()
-            block = (gu_rows if k == 0 else dn_cols)(back(d) * n_r + r)
-            for e in (1, 2, 3):
-                weights_b[d, e, k] = go(remote(block, block, s_b.at[d, e - 1, k], r_b.at[d, e - 1, k], h, beside(e), c))
-        if k == 0:
-            for d in (1, 3, 2):
-                acts[d].wait_recv()
-                block = rows_in.at[token_rows(back(d), c)]
-                peers[d] = go(remote(block, block, s_p.at[d], r_p.at[d], h, r, 1 - c))
+        across[e].wait_recv()
+
+    def part_of(ref, at, n):
+        logs = ref[at, heads * HD + n:heads * HD + n + 1, :].astype(f32) + ref[at, heads * HD + 8 + n:heads * HD + 9 + n, :].astype(f32)
+        return logs, ref[at, n * HD:(n + 1) * HD, :].astype(f32)
+
+    before = []
+    for n in range(heads):
+        whole = jnp.zeros((HD, HD), f32)
+        whole_log = jnp.zeros((1, HD), f32)
+        early, early_log = whole, whole_log
+        for at in range(n_r):
+            logs, state = part_of(plane, at, n)
+            whole = whole * jnp.exp(logs) + state
+            whole_log = whole_log + logs
+            early = jnp.where(at < r, whole, early)
+            early_log = jnp.where(at < r, whole_log, early_log)
+        before.append((early_log, early))
+        columns[h, n * HD:(n + 1) * HD, :] = whole.astype(bf)
+        high = whole_log.astype(bf)
+        columns[h, heads * HD + n:heads * HD + n + 1, :] = high
+        columns[h, heads * HD + 8 + n:heads * HD + 9 + n, :] = (whole_log - high.astype(f32)).astype(bf)
+    along = {d: go(remote(columns.at[h], columns.at[h], s_2.at[d - 1], r_2.at[d - 1], away(d), r, c)) for d in (1, 3, 2)}
+    hand_on(3, 0)
+    hand_on(2, 0)
+    share_out(1)
+    for d in (1, 3, 2):
+        along[d].wait_recv()
+    for n in range(heads):
+        cols = slice(n * HD, (n + 1) * HD)
+        state = jnp.zeros((HD, HD), f32)
+        for at in range(GROUPS - 1):
+            logs, later = part_of(columns, at, n)
+            state = jnp.where(at < h, state * jnp.exp(logs) + later, state)
+        early_log, early = before[n]
+        state = state * jnp.exp(early_log) + early
+        mixed = grown[:, cols] + over(q_grown[:, cols], state.astype(bf), 1, 1)
+        scale = lax.rsqrt(jnp.mean(mixed * mixed, axis=-1, keepdims=True) + eps)
+        gate = og_ref[:, cols].astype(f32)
+        gated[:, cols] = (mixed * scale * head_gain_ref[...] * (gate * jax.nn.sigmoid(gate))).astype(bf)
+
+    def project(j, carry):
+        at = pl.multiple_of(j * 256, 256)
+        proj[:, pl.ds(at, 256)] = jnp.dot(
+            gated[...], ow_ref[:, pl.ds(at, 256)], preferred_element_type=f32
+        ).astype(bf)
+        return carry
+
+    lax.fori_loop(0, model // 256, project, 0)
+    joined = go(remote(proj.at[theirs], proj_got, s_j.at[0], r_j.at[0], h, r, 1 - c))
+    joined.wait_recv()
+    x = (residual_ref[mine, :].astype(f32) + (proj[mine, :].astype(f32) + proj_got[...].astype(f32))).astype(bf)
+    x_own[...] = x
+    wide = x.astype(f32)
+    normed = wide * lax.rsqrt(jnp.mean(wide * wide, axis=-1, keepdims=True) + eps) * ff_gain_ref[...]
+    rows_in[token_rows(h, c), :] = normed.astype(bf)
+    block = rows_in.at[token_rows(h, c)]
+    acts = {d: go(remote(block, block, s_x.at[d - 1], r_x.at[d - 1], away(d), r, c)) for d in (1, 3, 2)}
+    peers = {0: go(remote(block, block, s_p.at[0], r_p.at[0], h, r, 1 - c))}
+    for d in (1, 3, 2):
+        hand_on(d, 1)
+    for d in (1, 3, 2):
+        acts[d].wait_recv()
+        block = rows_in.at[token_rows(back(d), c)]
+        peers[d] = go(remote(block, block, s_p.at[d], r_p.at[d], h, r, 1 - c))
     own_gu.wait()
     own_dn.wait()
     for d in range(4):
@@ -158,7 +257,7 @@
 
     def reduce_block(d, exchange):
         exchange.wait_recv()
-        here = part[d, pl.ds(pl.multiple_of(c * own, own), own), :]
+        here = part[d, mine, :]
         total = here.astype(jnp.float32) + peer_part[d].astype(jnp.float32)
         summed[d] = total.astype(jnp.bfloat16)
         if d == 0:
@@ -196,7 +295,7 @@
 
         lax.fori_loop(0, model // tile, down, 0)
         exchanges[d] = go(remote(
-            part.at[d, pl.ds(pl.multiple_of((1 - c) * own, own), own)], peer_part.at[d],
+            part.at[d, theirs], peer_part.at[d],
             s_d.at[d], r_d.at[d], h, r, 1 - c,
         ))
         if place:
@@ -206,55 +305,77 @@
     for d in (1, 3, 2):
         reduced[d].wait_recv()
         total = total + got[d - 1].astype(jnp.float32)
-    mine = pl.ds(pl.multiple_of(c * own, own), own)
-    out_ref[mine, :] = (x_ref[...].astype(jnp.float32) + 0.5 * total).astype(jnp.bfloat16)
+    out_ref[mine, :] = (x_own[...].astype(jnp.float32) + 0.5 * total).astype(jnp.bfloat16)
     finish = go(remote(out_ref.at[mine], out_ref.at[mine], s_o.at[0], r_o.at[0], h, r, 1 - c))
     finish.wait_recv()
     for copy in started:
         copy.wait_send()
 
 
-def feed_forward(gate_weight, up_weight, down_weight, after_mixer, normed):
+def layer(
+    residual, queries, forget_gate_logits, projected_values, output_gate_logits, lower_bound_margin,
+    extra_forget_logs, per_head_norm_gain, output_weight, feedforward_norm_gain, gate_weight, up_weight, down_weight,
+):
     n_sp = lax.axis_size("sp")
     share, half = gate_weight.shape
     width = half // GROUPS
     padded = up_to(width, 256)
-    own, model = normed.shape
+    length, model = residual.shape
+    own = length // 2
+    channels = queries.shape[1]
+    message = channels + 16
     pad = ((0, 0), (0, 0), (0, padded - width))
     split = lambda w: jnp.pad(w.reshape(share, GROUPS, width), pad)
     gu = jnp.concatenate([split(gate_weight), split(up_weight)], axis=2).transpose(1, 0, 2)
     dn = down_weight.reshape(GROUPS, width, share)
-    bf = jnp.bfloat16
+    bf, f32 = jnp.bfloat16, jnp.float32
     dma = pltpu.SemaphoreType.DMA
-    dims = (n_sp // GROUPS, share, own, width, padded)
+    n_r = n_sp // GROUPS
+    dims = (n_r, share, own, width, padded)
     vm = pl.BlockSpec(memory_space=pltpu.VMEM)
     hbm = pl.BlockSpec(memory_space=pl.ANY)
     return pl.pallas_call(
-        lambda *refs: feed_forward_kernel(dims, *refs),
-        out_shape=jax.ShapeDtypeStruct((2 * own, model), bf),
-        in_specs=[hbm, hbm, vm, vm],
+        lambda *refs: layer_kernel(dims, *refs),
+        out_shape=jax.ShapeDtypeStruct((length, model), bf),
+        in_specs=[hbm, hbm] + [vm] * 10,
         out_specs=vm,
         scratch_shapes=[
             pltpu.VMEM((model, 2 * padded), bf),
             pltpu.VMEM((padded, model), bf),
-            pltpu.VMEM((GROUPS * 2 * own, model), bf),
-            pltpu.VMEM((2 * own, padded), bf),
-            pltpu.VMEM((GROUPS, 2 * own, model), bf),
+            pltpu.VMEM((length, channels), f32),
+            pltpu.VMEM((length, channels), bf),
+            pltpu.VMEM((n_r, message, HD), bf),
+            pltpu.VMEM((GROUPS, message, HD), bf),
+            pltpu.VMEM((length, channels), bf),
+            pltpu.VMEM((length, model), bf),
+            pltpu.VMEM((own, model), bf),
+            pltpu.VMEM((own, model), bf),
+            pltpu.VMEM((GROUPS * length, model), bf),
+            pltpu.VMEM((length, padded), bf),
+            pltpu.VMEM((GROUPS, length, model), bf),
             pltpu.VMEM((GROUPS, own, model), bf),
             pltpu.VMEM((GROUPS, own, model), bf),
             pltpu.VMEM((GROUPS - 1, own, model), bf),
             dma((3, 2)), dma((3, 2)), dma((4, 3, 2)), dma((4, 3, 2)),
             dma((3,)), dma((3,)), dma((4,)), dma((4,)), dma((4,)), dma((4,)),
             dma((3,)), dma((3,)), dma((1,)), dma((1,)), dma((2,)),
+            dma((3,)), dma((3,)), dma((3,)), dma((3,)), dma((1,)), dma((1,)),
         ],
         compiler_params=pltpu.CompilerParams(has_side_effects=True, vmem_limit_bytes=56 * 2**20),
-    )(gu, dn, after_mixer, normed)
-
-
-def fits(mesh, share, own, width):
+    )(
+        gu, dn, queries, forget_gate_logits, projected_values, output_gate_logits,
+        lower_bound_margin.reshape(1, channels), extra_forget_logs, per_head_norm_gain.reshape(1, HD),
+        output_weight, residual, feedforward_norm_gain.reshape(1, model),
+    )
+
+
+def fits(residual, queries, gate_weight):
+    length, model = residual.shape
+    share, half = gate_weight.shape
     return (
-        mesh["sp"] == 4 * GROUPS and mesh["tp"] == 2
-        and share % 128 == 0 and own % 16 == 0 and width % 16 == 0
+        lax.axis_size("sp") == 4 * GROUPS and lax.axis_size("tp") == 2 and share % 128 == 0
+        and length % 128 == 0 and length <= 512 and half % (16 * GROUPS) == 0
+        and queries.shape[1] <= 8 * HD and model % 256 == 0
     )
 
 
@@ -273,6 +394,11 @@
     up_weight,
     down_weight,
 ):
+    if fits(residual, queries, gate_weight):
+        return layer(
+            residual, queries, forget_gate_logits, projected_values, output_gate_logits, lower_bound_margin,
+            extra_forget_logs, per_head_norm_gain, output_weight, feedforward_norm_gain, gate_weight, up_weight, down_weight,
+        )
     length = queries.shape[0]
     head_count = queries.shape[1] // HD
     state_increment = lower_bound_margin * jax.nn.sigmoid(-forget_gate_logits.astype(jnp.float32))
@@ -323,9 +449,6 @@
         * lax.rsqrt(jnp.mean(widened * widened, axis=-1, keepdims=True) + eps)
         * feedforward_norm_gain
     ).astype(jnp.bfloat16)
-    sizes = {"sp": lax.axis_size("sp"), "tp": lax.axis_size("tp")}
-    if fits(sizes, gate_weight.shape[0], row_count, gate_weight.shape[1] // GROUPS):
-        return feed_forward(gate_weight, up_weight, down_weight, after_mixer, normed)
     gate_full, up_full = (
         lax.all_gather(gate_weight, "sp", axis=0, tiled=True),
         lax.all_gather(up_weight, "sp", axis=0, tiled=True),

time: 379 us -> 183 us (0.48)
  matrix products: 68.6 us -> 0 us
  blocking collectives: 42.6 us -> 0 us
  waiting for transfers between devices: 35.5 us -> 0 us
  local copies, waits for them, and re-layouts: 24 us -> 4.75 us
  between operations: 13.5 us -> 0.03 us
  other arithmetic: 11.4 us -> 1.3 us
  Pallas kernels: 182 us -> 177 us
    dot_general x18 -> x0, matrix products: 68.6 us -> none  [the longest x4 56.2 us: block_update(): jnp.einsum('htk,htsk,hsk->hts', queries, weights, state_increment, precis...]
    all_gather x1 -> x0, blocking collectives: 42.6 us -> none  [carried_in_2(): lax.all_gather(a.astype(kind), axis)]
    all_gather x1 -> x0, waiting for transfers between devices: 20.7 us -> none  [carried_in_2(): lax.all_gather(a.astype(kind), axis)]
    reduce_scatter x1 -> x0, waiting for transfers between devices: 14.8 us -> none  [local(): lax.psum_scatter(jnp.dot(rows_here, output_weight, preferred_element_type...]
    dynamic_slice x20 -> x0, local copies, waits for them, and re-layouts: 7.77 us -> none  [local(): lax.scan(block_update, initial, block_inputs)]
    reshape x4 -> x2, local copies, waits for them, and re-layouts: 5.83 us -> 0.57 us  [layer(): split = lambda w: jnp.pad(w.reshape(share, GROUPS, width), pad)]
    pallas_call x1, Pallas kernels: 182 us -> 177 us  [layer(): pl.pallas_call(lambda *refs: layer_kernel(dims, *refs), out_shape=jax.Sha...]
    transpose x3 -> x0, local copies, waits for them, and re-layouts: 4.18 us -> none  [the longest x2 3.83 us: to_blocks(): source.reshape(length // BLOCK, BLOCK, head_count, HD).transpose(0, 2, 1, 3)]
  transfers between devices with their start and end apart: 2 -> 0, of which waited for: 2 -> 0; matrix products, arithmetic and copies ran while one was open for 3% -> 0% of each run, Pallas kernels for 0% -> 0%
where the time goes in v2:
time: 183 us
  Pallas kernels  177 us (97%)
  local copies, waits for them, and re-layouts  4.75 us (3%)
    pallas_call x1, Pallas kernels, layer(): pl.pallas_call(lambda *refs: layer_kernel(dims, *refs), out_shape=jax.Sha...  177 us
    unnamed x5, local copies, waits for them, and re-layouts  4.18 us

profile of v2, /device:TPU:0, one launch (start us, length us, event | category | flops | bytes accessed | tf_op | source)
XLA Modules:
  0.0 183.3 jit_solution(8139907193895051749)
XLA Ops:
  0.0 0.0 copy-start
  0.0 1.5 copy.14
  1.5 0.3 copy.15
  1.8 0.0 copy-done
  1.8 0.3 copy.16
  2.2 0.3 copy.17
  2.5 1.3 fusion.3.refs_0_
  3.8 177.2 %shard_map.127 = bf16[256,2048]{1,0:T(8,128)(2,1)} custom-call(bf16[4,128,1536]{2,1,0:T(8,128)(2,1)} %fusion.3.refs_0_, bf16[4,704,128]{2,1,0:T(8,128)(2,1)} %bitcast.10, bf16[256,512]{1,0:T(8,128)(2,1)} %refs_2_.1, bf16[256,512]{1,0:T(8,128)(2,1)} %refs_3_.1, bf16[256,512]{1,0:T(8,128)(2,1)} %refs_4_.1, bf16[256,512]{1,0:T(8,128)(2,1)} %refs_5_.1, ...), custom_call_target="tpu_custom_call" | custom-call | tf_op jit(solution)/shard_map/pallas_call | solution.py:337
  181.0 2.3 %copy.19 = bf16[256,2048]{1,0:T(8,128)(2,1)} copy(bf16[256,2048]{1,0:T(8,128)(2,1)} %shard_map.127) | data formatting | bytes 2097152
Async XLA Ops:
  0.0 1.8 copy-start

commit v3 on v2

--- a/solution.py
+++ b/solution.py
@@ -130,21 +130,35 @@
         place = (gu_rows, dn_cols)[k]
         for d in (1, 3, 2):
             weights_a[d, k] = go(remote(source.at[away(d)], place(me), s_a.at[d - 1, k], r_a.at[d - 1, k], away(d), r, c))
-        for e in (1, 2, 3):
+        for e in (1, 2):
             weights_b[0, e, k] = go(remote(source.at[h], place(me), s_b.at[0, e - 1, k], r_b.at[0, e - 1, k], h, beside(e), c))
 
     def hand_on(d, k):
         weights_a[d, k].wait_recv()
         block = (gu_rows, dn_cols)[k](back(d) * n_r + r)
-        for e in (1, 2, 3):
+        for e in (1, 2):
             weights_b[d, e, k] = go(remote(block, block, s_b.at[d, e - 1, k], r_b.at[d, e - 1, k], h, beside(e), c))
+
+    here_already = set()
+
+    def arrive(*key):
+        if key not in here_already:
+            here_already.add(key)
+            weights_b[key].wait_recv()
+
+    def relay(d, k):
+        first = 1 + d % 2
+        arrive(d, first, k)
+        block = (gu_rows, dn_cols)[k](back(d) * n_r + beside(first))
+        weights_b[d, 3, k] = go(remote(block, block, s_b.at[d, 2, k], r_b.at[d, 2, k], h, beside(3 - first), c))
 
     share_out(0)
     own_gu = pltpu.make_async_copy(gu_ref.at[h], gu_rows(me), s_l.at[0])
     own_dn = pltpu.make_async_copy(dn_ref.at[h], dn_cols(me), s_l.at[1])
     own_gu.start()
     own_dn.start()
-    dn[pl.ds(width, padded - width), :] = jnp.zeros((padded - width, model), dn.dtype)
+    if padded > width:
+        dn[pl.ds(width, padded - width), :] = jnp.zeros((padded - width, model), dn.dtype)
 
     bf, f32 = jnp.bfloat16, jnp.float32
     length, channels = q_ref.shape
@@ -182,6 +196,7 @@
         plane[r, heads * HD + 8 + n:heads * HD + 9 + n, :] = (base - high.astype(f32)).astype(bf)
 
     across = {e: go(remote(plane.at[r], plane.at[r], s_1.at[e - 1], r_1.at[e - 1], h, beside(e), c)) for e in (1, 2, 3)}
+    relay(0, 0)
     hand_on(1, 0)
     for e in (1, 2, 3):
         across[e].wait_recv()
@@ -208,6 +223,7 @@
         columns[h, heads * HD + 8 + n:heads * HD + 9 + n, :] = (whole_log - high.astype(f32)).astype(bf)
     along = {d: go(remote(columns.at[h], columns.at[h], s_2.at[d - 1], r_2.at[d - 1], away(d), r, c)) for d in (1, 3, 2)}
     hand_on(3, 0)
+    relay(1, 0)
     hand_on(2, 0)
     share_out(1)
     for d in (1, 3, 2):
@@ -243,8 +259,14 @@
     block = rows_in.at[token_rows(h, c)]
     acts = {d: go(remote(block, block, s_x.at[d - 1], r_x.at[d - 1], away(d), r, c)) for d in (1, 3, 2)}
     peers = {0: go(remote(block, block, s_p.at[0], r_p.at[0], h, r, 1 - c))}
+    relay(3, 0)
+    hand_on(1, 1)
+    relay(2, 0)
+    hand_on(3, 1)
+    relay(0, 1)
+    hand_on(2, 1)
     for d in (1, 3, 2):
-        hand_on(d, 1)
+        relay(d, 1)
     for d in (1, 3, 2):
         acts[d].wait_recv()
         block = rows_in.at[token_rows(back(d), c)]
@@ -253,7 +275,7 @@
     own_dn.wait()
     for d in range(4):
         for e in (1, 2, 3):
-            weights_b[d, e, 0].wait_recv()
+            arrive(d, e, 0)
 
     def reduce_block(d, exchange):
         exchange.wait_recv()
@@ -273,18 +295,22 @@
         first = pl.multiple_of(back(d) * 2 * own, 2 * own)
 
         def gate_up(j, carry):
-            at = pl.multiple_of(j * tile, tile)
-            rows = rows_in[pl.ds(first, 2 * own), :]
-            gate = jnp.dot(rows, gu[:, pl.ds(at, tile)], preferred_element_type=jnp.float32)
-            up = jnp.dot(rows, gu[:, pl.ds(padded + at, tile)], preferred_element_type=jnp.float32)
-            hid[:, pl.ds(at, tile)] = (gate * jax.nn.sigmoid(gate) * up).astype(jnp.bfloat16)
+            at = pl.multiple_of(j * 256, 256)
+            both = jnp.dot(rows_in[pl.ds(first, 2 * own), :], gu[:, pl.ds(at, 256)], preferred_element_type=jnp.float32)
+            gate, up = both[:, :128], both[:, 128:]
+            hid[:, pl.ds(pl.multiple_of(j * 128, 128), 128)] = (gate * jax.nn.sigmoid(gate) * up).astype(jnp.bfloat16)
             return carry
 
-        lax.fori_loop(0, padded // tile, gate_up, 0)
+        lax.fori_loop(0, width // 128, gate_up, 0)
+        if width % 128:
+            both = jnp.dot(
+                rows_in[pl.ds(first, 2 * own), :], gu[:, 2 * (width // 128 * 128):], preferred_element_type=jnp.float32
+            )
+            hid[:, width // 128 * 128:] = (both * jax.nn.sigmoid(both) * pltpu.roll(both, 64, 1)).astype(jnp.bfloat16)
         if place == 0:
             for dd in range(4):
                 for e in (1, 2, 3):
-                    weights_b[dd, e, 1].wait_recv()
+                    arrive(dd, e, 1)
 
         def down(j, carry):
             at = pl.multiple_of(j * tile, tile)
@@ -312,6 +338,18 @@
         copy.wait_send()
 
 
+def interleave_kernel(width, gate_ref, up_ref, out_ref):
+    even = width // 128 * 128
+    for group in range(GROUPS):
+        first = group * width
+        gate, up = gate_ref[:, first:first + width], up_ref[:, first:first + width]
+        for at in range(0, even, 128):
+            out_ref[group, :, 2 * at:2 * at + 128] = gate[:, at:at + 128]
+            out_ref[group, :, 2 * at + 128:2 * at + 256] = up[:, at:at + 128]
+        if width > even:
+            out_ref[group, :, 2 * even:] = jnp.concatenate([gate[:, even:], up[:, even:]], axis=1)
+
+
 def layer(
     residual, queries, forget_gate_logits, projected_values, output_gate_logits, lower_bound_margin,
     extra_forget_logs, per_head_norm_gain, output_weight, feedforward_norm_gain, gate_weight, up_weight, down_weight,
@@ -319,14 +357,15 @@
     n_sp = lax.axis_size("sp")
     share, half = gate_weight.shape
     width = half // GROUPS
-    padded = up_to(width, 256)
+    padded = up_to(width, 128)
     length, model = residual.shape
     own = length // 2
     channels = queries.shape[1]
     message = channels + 16
-    pad = ((0, 0), (0, 0), (0, padded - width))
-    split = lambda w: jnp.pad(w.reshape(share, GROUPS, width), pad)
-    gu = jnp.concatenate([split(gate_weight), split(up_weight)], axis=2).transpose(1, 0, 2)
+    gu = pl.pallas_call(
+        lambda *refs: interleave_kernel(width, *refs),
+        out_shape=jax.ShapeDtypeStruct((GROUPS, share, 2 * width), jnp.bfloat16),
+    )(gate_weight, up_weight)
     dn = down_weight.reshape(GROUPS, width, share)
     bf, f32 = jnp.bfloat16, jnp.float32
     dma = pltpu.SemaphoreType.DMA
@@ -340,7 +379,7 @@
         in_specs=[hbm, hbm] + [vm] * 10,
         out_specs=vm,
         scratch_shapes=[
-            pltpu.VMEM((model, 2 * padded), bf),
+            pltpu.VMEM((model, 2 * width), bf),
             pltpu.VMEM((padded, model), bf),
             pltpu.VMEM((length, channels), f32),
             pltpu.VMEM((length, channels), bf),
@@ -374,7 +413,7 @@
     share, half = gate_weight.shape
     return (
         lax.axis_size("sp") == 4 * GROUPS and lax.axis_size("tp") == 2 and share % 128 == 0
-        and length % 128 == 0 and length <= 512 and half % (16 * GROUPS) == 0
+        and length % 128 == 0 and length <= 512 and half % (64 * GROUPS) == 0
         and queries.shape[1] <= 8 * HD and model % 256 == 0
     )
 

time: 183 us -> 180 us (0.984)
  local copies, waits for them, and re-layouts: 4.75 us -> 2.3 us
    pallas_call x0 -> x1, Pallas kernels: none -> 2.8 us  [layer(): pl.pallas_call(lambda *refs: interleave_kernel(width, *refs), out_shape=j...]
    pallas_call x1, Pallas kernels: 177 us -> 175 us  [layer(): pl.pallas_call(lambda *refs: layer_kernel(dims, *refs), out_shape=jax.Sha...]
    unnamed x5 -> x1, local copies, waits for them, and re-layouts: 4.18 us -> 2.3 us
where the time goes in v3:
time: 180 us
  Pallas kernels  178 us (99%)
  local copies, waits for them, and re-layouts  2.3 us (1%)
    pallas_call x1, Pallas kernels, layer(): pl.pallas_call(lambda *refs: layer_kernel(dims, *refs), out_shape=jax.Sha...  175 us

profile of v3, /device:TPU:0, one launch (start us, length us, event | category | flops | bytes accessed | tf_op | source)
XLA Modules:
  0.0 180.1 jit_solution(18033743067022472007)
XLA Ops:
  0.0 2.8 %shard_map.127.refs_0_ = bf16[4,128,1408]{2,1,0:T(8,128)(2,1)} custom-call(bf16[128,2816]{1,0:T(8,128)(2,1)} %refs_0_.1, bf16[128,2816]{1,0:T(8,128)(2,1)} %refs_1_.1), custom_call_target="tpu_custom_call" | custom-call | tf_op jit(solution)/shard_map/pallas_call | solution.py:365
  2.8 175.0 %shard_map.128 = bf16[256,2048]{1,0:T(8,128)(2,1)} custom-call(bf16[4,128,1408]{2,1,0:T(8,128)(2,1)} %shard_map.127.refs_0_, bf16[4,704,128]{2,1,0:T(8,128)(2,1)} %bitcast.4, bf16[256,512]{1,0:T(8,128)(2,1)} %refs_2_.1, bf16[256,512]{1,0:T(8,128)(2,1)} %refs_3_.1, bf16[256,512]{1,0:T(8,128)(2,1)} %refs_4_.1, bf16[256,512]{1,0:T(8,128)(2,1)} %refs_5_.1, ...), custom_call_target="tpu_custom_call" | custom-call | tf_op jit(solution)/shard_map/pallas_call | solution.py:376
  177.8 2.3 %copy.15 = bf16[256,2048]{1,0:T(8,128)(2,1)} copy(bf16[256,2048]{1,0:T(8,128)(2,1)} %shard_map.128) | data formatting | bytes 2097152
